TPU v7x, 32 devices: a whole 2x2x4 slice. The times are simulated.
32 devices in a mesh: ep: 8 (over z, core), tp: 4 (over y, x).
Axes of the slice: x: 2, y: 2, z: 4, core: 2. Of those that a mesh axis runs over, the one named last changes fastest.
Arguments:
- query_rows: bfloat16 [3072, 2048], P('ep', 'tp'), may hold values from -6 to 6
- key_rows: bfloat16 [3072, 2048], P('ep', 'tp'), may hold values from -6 to 6
- value_rows: bfloat16 [3072, 2048], P('ep', 'tp'), may hold values from -6 to 6
- second_scale: float32 [16], P('tp'), may hold values from 0.3 to 0.8
- head_gain: float32 [128], replicated, may hold values from 0.1 to 1.9
- out_weight: bfloat16 [2048, 4096], P(None, 'tp'), may hold values from -0.125 to 0.125
- routed_rows: bfloat16 [1024, 4096], P('ep', 'tp'), may hold values from -6 to 6
- norm_gain: float32 [4096], replicated, may hold values from 0.1 to 1.9
- route_ids: int32 [1024, 2], P('ep'), may hold values from 0 to 7, all different within a row; in each aligned block of 128 rows (0 to 127, 128 to 255, ...) at most 64 rows name the same one
- route_weight: float32 [1024, 2], P('ep'), may hold values from 0.1 to 0.9
- expert_gate: bfloat16 [8, 4096, 2048], P('ep', None, 'tp'), may hold values from -0.09375 to 0.09375
- expert_up: bfloat16 [8, 4096, 2048], P('ep', None, 'tp'), may hold values from -0.09375 to 0.09375
- expert_down: bfloat16 [8, 2048, 4096], P('ep', None, 'tp'), may hold values from -0.125 to 0.125
Outputs:
- mixer_out: bfloat16 [3072, 4096], P('ep', 'tp')
- expert_mix: bfloat16 [1024, 4096], P('ep', 'tp')
Inputs may be any that keep to these rules, and one draw needn't show every extreme that they name: `route_ids`: among the 128 tokens of one index of ep, no expert is named by more than 64 of them, a bound that some block reaches.
All inputs are finite; a program needn't handle non-finite values.
Results may differ from a plain program's by a relative error of at most 0.0085.
Values may be sent and summed in bfloat16 or wider, within the bound.
No kernel may reach another device: no remote copies, remote signals or barrier semaphores. Data moves between devices by JAX's collectives and lax.ppermute only.
A program may use at most 128 MiB of HBM per device.

v0:
```python
import jax
import jax.numpy as jnp
from jax import lax
from jax.sharding import PartitionSpec as P

eps = 1e-06
head_factor = 0.8
neg_big = -1e30
key_block_rows = 1024


def rms_rows(rows_in, gain):
    floats = rows_in.astype(jnp.float32)
    factor = lax.rsqrt(jnp.mean(floats * floats, axis=-1, keepdims=True) + eps)
    return (floats * factor * gain).astype(jnp.bfloat16)


def per_device(
    query_rows,
    key_rows,
    value_rows,
    second_scale,
    head_gain,
    out_weight,
    routed_rows,
    norm_gain,
    route_ids,
    route_weight,
    expert_gate,
    expert_up,
    expert_down,
):
    count_a = query_rows.shape[0]
    per_head = second_scale.shape[0]
    head_dim = query_rows.shape[1] // (2 * per_head)
    value_dim = head_gain.shape[0]
    query_four = query_rows.reshape(count_a, per_head, 2, head_dim)
    query_pos = lax.axis_index("ep") * count_a + jnp.arange(count_a, dtype=jnp.int32)

    def key_block(carry_state, key_part, value_part, block_start):
        key_count = key_part.shape[0]
        key_four = key_part.reshape(key_count, per_head, 2, head_dim)
        value_three = value_part.reshape(key_count, per_head, value_dim)
        scores = jnp.einsum(
            "ihcd,jhcd->ihcj", query_four, key_four, preferred_element_type=jnp.float32
        ) * head_dim ** (-0.5)
        allowed = (
            query_pos[:, None] >= block_start + jnp.arange(key_count, dtype=jnp.int32)[None, :]
        )[:, None, None, :]
        scores = jnp.where(allowed, scores, neg_big)
        old_max, old_sum, old_acc = carry_state
        new_max = jnp.maximum(old_max, jnp.max(scores, axis=-1))
        weights = jnp.where(allowed, jnp.exp(scores - new_max[..., None]), 0.0)
        shrink = jnp.exp(old_max - new_max)
        new_sum = old_sum * shrink + jnp.sum(weights, axis=-1)
        update = jnp.einsum(
            "ihcj,jhe->ihce",
            weights.astype(jnp.bfloat16),
            value_three,
            preferred_element_type=jnp.float32,
        )
        return (new_max, new_sum, old_acc * shrink[..., None] + update)

    start_state = (
        jnp.full((count_a, per_head, 2), neg_big, jnp.float32),
        jnp.zeros((count_a, per_head, 2), jnp.float32),
        jnp.zeros((count_a, per_head, 2, value_dim), jnp.float32),
    )
    key_part = lax.all_gather(key_rows, "ep", axis=0, tiled=True)
    value_part = lax.all_gather(value_rows, "ep", axis=0, tiled=True)
    key_count = key_part.shape[0]

    def step_block(block_num, inner_state):
        offset_rows = block_num * key_block_rows
        key_slice = lax.dynamic_slice_in_dim(key_part, offset_rows, key_block_rows, 0)
        value_slice = lax.dynamic_slice_in_dim(value_part, offset_rows, key_block_rows, 0)
        return key_block(inner_state, key_slice, value_slice, offset_rows)

    run_max, run_sum, run_acc = lax.fori_loop(
        0, key_count // key_block_rows, step_block, start_state
    )
    maps_both = run_acc / run_sum[..., None]
    mixed_maps = maps_both[:, :, 0] - second_scale[None, :, None] * maps_both[:, :, 1]
    mean_sq = jnp.mean(mixed_maps * mixed_maps, axis=-1, keepdims=True)
    head_out = (
        (mixed_maps * lax.rsqrt(mean_sq + eps) * head_gain * head_factor)
        .astype(jnp.bfloat16)
        .reshape(count_a, per_head * value_dim)
    )
    count_b = routed_rows.shape[0]
    route_count = route_ids.shape[1]
    experts_here = expert_gate.shape[0]
    ep_devices = lax.axis_size("ep")
    expert_total = experts_here * ep_devices
    capacity = 2 * count_b * route_count // expert_total
    flat_expert = route_ids.reshape(-1)
    chosen = (flat_expert[:, None] == jnp.arange(expert_total, dtype=jnp.int32)[None, :]).astype(
        jnp.int32
    )
    ranks = jnp.sum((jnp.cumsum(chosen, axis=0) - 1) * chosen, axis=1)
    slot_of = flat_expert * capacity + ranks
    token_of = jnp.arange(count_b * route_count, dtype=jnp.int32) // route_count
    slot_token = jnp.full((expert_total * capacity,), count_b, jnp.int32).at[slot_of].set(token_of)
    padded = jnp.concatenate(
        [routed_rows, jnp.zeros((1, routed_rows.shape[1]), jnp.bfloat16)], axis=0
    )
    outgoing = padded[slot_token].reshape(ep_devices, experts_here, capacity, routed_rows.shape[1])
    column_parts = lax.all_to_all(outgoing, "ep", split_axis=0, concat_axis=0, tiled=True)
    arrived = rms_rows(lax.all_gather(column_parts, "tp", axis=3, tiled=True), norm_gain)
    gate_val = jnp.einsum(
        "sxcd,xdf->sxcf", arrived, expert_gate, preferred_element_type=jnp.float32
    )
    up_val = jnp.einsum("sxcd,xdf->sxcf", arrived, expert_up, preferred_element_type=jnp.float32)
    hidden = (jax.nn.silu(gate_val) * up_val).astype(jnp.bfloat16)
    weight_rows = out_weight
    attn_total = jnp.dot(
        lax.all_gather(
            head_out.reshape(1, 1, count_a, head_out.shape[1]), "tp", axis=3, tiled=True
        )[0, 0],
        weight_rows,
        preferred_element_type=jnp.float32,
    )
    weight_rows = expert_down
    moe_total = jnp.einsum(
        "sxcf,xfd->sxcd",
        lax.all_gather(hidden, "tp", axis=3, tiled=True),
        weight_rows,
        preferred_element_type=jnp.float32,
    )
    mixer_out = attn_total.astype(jnp.bfloat16)
    returned = lax.all_to_all(
        moe_total.astype(jnp.bfloat16), "ep", split_axis=0, concat_axis=0, tiled=True
    )
    flat_back = returned.reshape(expert_total * capacity, returned.shape[3])
    picked = flat_back[slot_of].astype(jnp.float32).reshape(count_b, route_count, returned.shape[3])
    expert_mix = jnp.sum(picked * route_weight[:, :, None], axis=1).astype(jnp.bfloat16)
    return (mixer_out, expert_mix)


def solution(mesh):
    placed = (
        P("ep", "tp"),
        P("ep", "tp"),
        P("ep", "tp"),
        P("tp"),
        P(),
        P(None, "tp"),
        P("ep", "tp"),
        P(),
        P("ep", None),
        P("ep", None),
        P("ep", None, "tp"),
        P("ep", None, "tp"),
        P("ep", None, "tp"),
    )
    return jax.shard_map(
        per_device,
        mesh=mesh,
        in_specs=placed,
        out_specs=(P("ep", "tp"), P("ep", "tp")),
        check_vma=False,
    )
```

profile of v0, /device:TPU:0, one launch (start us, length us, event | category | flops | bytes accessed | tf_op | source)
XLA Modules:
  0.0 287.7 jit_solution(6418652989304294273)
XLA Ops:
  7.2 0.0 all-gather.12.cloned.1.call-start
  7.2 0.7 broadcast_multiply_fusion
  7.9 0.8 copy.36
  8.7 0.1 eq.29
  8.8 0.1 eq.25
  9.0 0.1 copy.35
  9.1 0.1 mul.194
  9.2 0.6 reduce-window.6
  9.8 0.2 slice_reduce_fusion
  10.1 0.1 fusion.65
  10.2 1.4 scatter_custom_fusion
  11.6 1.0 concatenate.3
  12.6 2.1 gather_fusion
  14.7 33.0 %all_to_all.10 = bf16[8,1,64,1024]{3,2,1,0:T(8,128)(2,1)} all-to-all(bf16[8,1,64,1024]{3,2,1,0:T(8,128)(2,1)S(1)} %bitcast.152), channel_id=1, replica_groups=mesh['ep'=8,'tp'=4] {'ep'}, dimensions={0} | all-to-all | bytes 2097152 | tf_op jit(solution)/shard_map/all_to_all | solution.py:108
  47.7 0.0 all-gather.12.cloned.1.call-update
  47.7 0.0 all-gather.6.cloned.1.call-start
  47.7 0.9 copy.31
  48.7 0.0 all-gather.8.cloned.1.call-start
  48.8 0.9 copy.33
  49.7 0.0 all-gather.14.cloned.1.call-start
  49.8 1.2 copy.32
  51.0 0.1 broadcast_bitcast_fusion
  51.1 48.2 %all-gather.12.cloned.1.call-done = bf16[8,1,64,4096]{3,2,1,0:T(8,128)(2,1)} async-done(((bf16[8,1,64,1024]{3,2,1,0:T(8,128)(2,1)}), bf16[8,1,64,4096]{3,2,1,0:T(8,128)(2,1)}) %all-gather.12.cloned.1.call-update) | async-done | bytes 4194320 | tf_op jit(solution)/shard_map/all_gather | solution.py:109
  99.4 3.2 %fusion.15 = f32[8,64]{1,0:T(8,128)S(1)} fusion(bf16[8,1,64,4096]{3,2,1,0:T(8,128)(2,1)} %all-gather.12.cloned.1.call-done), kind=kLoop, calls=%fused_computation.28 | loop fusion | flops 6290944 | bytes 4196352 | tf_op jit(solution)/shard_map/reduce_sum | solution.py:14
  102.6 0.2 copy-done.1
  102.8 4.7 %fusion.43 = f32[8,1,64,512]{3,2,0,1:T(8,128)S(1)} fusion(bf16[1,4096,512]{2,1,0:T(8,128)(2,1)} %param.25, bf16[8,1,64,4096]{3,2,1,0:T(8,128)(2,1)S(1)} %copy-done.1, f32[4096]{0:T(1024)S(1)} %copy-done.8, f32[8,64]{1,0:T(8,128)S(1)} %add_rsqrt_fusion.1), kind=kOutput, calls=%fused_computation.44 | convolution fusion | flops 2155872256 | bytes 9455616 | tf_op jit(solution)/shard_map/sxcd,xdf->sxcf/dot_general | solution.py:110
  107.5 3.3 %fusion.58 = bf16[8,1,64,512]{3,2,0,1:T(8,128)(2,1)} fusion(bf16[1,4096,512]{2,1,0:T(8,128)(2,1)S(1)} %copy-done.7, bf16[8,1,64,4096]{3,2,1,0:T(8,128)(2,1)S(1)} %copy-done.1, f32[4096]{0:T(1024)S(1)} %copy-done.8, f32[8,64]{1,0:T(8,128)S(1)} %add_rsqrt_fusion.1, f32[8,1,64,512]{3,2,0,1:T(8,128)S(1)} %fusion.43), kind=kOutput, calls=%fused_computation.47 | convolution fusion | flops 2157445120 | bytes 9979904 | tf_op jit(solution)/shard_map/sxcd,xdf->sxcf/dot_general | solution.py:113
  110.8 0.2 all-gather.10.cloned.1.call-start
  111.0 27.7 %all-gather.6.cloned.1.call-done = bf16[3072,512]{0,1:T(8,128)(2,1)} async-done(((bf16[384,512]{0,1:T(8,128)(2,1)}), bf16[3072,512]{0,1:T(8,128)(2,1)}) %all-gather.6.cloned.1.call-update) | async-done | bytes 3145744 | tf_op jit(solution)/shard_map/all_gather | solution.py:69
  138.8 38.8 %all-gather.8.cloned.1.call-done = bf16[3072,512]{0,1:T(8,128)(2,1)} async-done(((bf16[384,512]{0,1:T(8,128)(2,1)}), bf16[3072,512]{0,1:T(8,128)(2,1)}) %all-gather.8.cloned.1.call-update) | async-done | bytes 3145744 | tf_op jit(solution)/shard_map/all_gather | solution.py:70
  177.5 61.9 %while.18 = (s32[]{:T(128)}, f32[384,4,2]{0,2,1:T(2,128)S(1)}, f32[384,4,2]{0,2,1:T(2,128)S(1)}, f32[384,4,2,128]{0,3,2,1:T(8,128)S(1)}, bf16[3072,512]{0,1:T(8,...) while((s32[]{:T(128)}, f32[384,4,2]{0,2,1:T(2,128)S(1)}, ...), condition=%wide.region_3.4_spmd.clone, body=%wide.region_0.3_spmd.clone.sunk | while | flops 1250443648 | bytes 99691744 | solution.py:79
  177.5 0.3 broadcast_compare_fusion.2
  177.8 1.7 constant_dynamic-slice_fusion.3
  179.5 6.7 %fusion.86 = (f32[384,4,2]{0,2,1:T(2,128)S(1)}, f32[4,2,1024,384]{3,2,1,0:T(8,128)}) fusion(pred[384,1024]{0,1:T(8,128)(4,1)S(1)} %broadcast_compare_fusion.2, bf16[1024,4,2,64]{0,3,2,1:T(8,128)(2,1)S(1)} %bitcast.148, bf16[384,4,2,64]{0,3,2,1:T(8,128)(2,1)S(1)} %get-tuple-element.290), kind=kOutput, calls=%fused_computation.6.clone.1 | convolution fusion | flops 412087296 | bytes 14430208 | tf_op jit(solution)/shard_map/while/body/eval_jaxpr/ihcd,jhcd->ihcj/dot_general | solution.py:44
  186.2 7.0 %fusion.88 = f32[384,4,2]{0,2,1:T(2,128)S(1)} fusion(f32[4,2,1024,384]{3,2,1,0:T(8,128)} %get-tuple-element.257, f32[384,4,2]{0,2,1:T(2,128)S(1)} %fusion.87, pred[384,1024]{0,1:T(8,128)(4,1)S(1)} %broadcast_compare_fusion.2), kind=kLoop, calls=%fused_computation.8.clone.1 | loop fusion | flops 15725568 | bytes 13000704 | tf_op jit(solution)/shard_map/while/body/eval_jaxpr/reduce_sum | solution.py:55
  193.2 1.5 copy-done
  194.7 3.6 %bitcast_add_fusion.2 = f32[384,4,2,128]{0,3,2,1:T(8,128)S(1)} fusion(f32[384,4,2,128]{0,3,2,1:T(8,128)S(1)} %get-tuple-element.276, bf16[1024,4,128,1]{0,2,3,1:T(8,128)(2,1)S(1)} %bitcast.149, f32[4,2,1024,384]{3,2,1,0:T(8,128)S(1)} %copy-done, f32[384,4,2]{0,2,1:T(2,128)S(1)} %fusion.87, pred[384,1024]{0,1:T(8,128)(4,1)S(1)} %broadcast_compare_fusion.2, ...), kind=kOutput, calls=%fused_computation.11.clone.1 | convolution fusion | flops 822214656 | bytes 17195008 | tf_op jit(solution)/shard_map/while/body/eval_jaxpr/ihcj,jhe->ihce/dot_general | solution.py:56
  198.3 0.3 broadcast_compare_fusion.2
  198.6 1.7 constant_dynamic-slice_fusion.3
  200.3 6.7 %fusion.86 = (f32[384,4,2]{0,2,1:T(2,128)S(1)}, f32[4,2,1024,384]{3,2,1,0:T(8,128)}) fusion(pred[384,1024]{0,1:T(8,128)(4,1)S(1)} %broadcast_compare_fusion.2, bf16[1024,4,2,64]{0,3,2,1:T(8,128)(2,1)S(1)} %bitcast.148, bf16[384,4,2,64]{0,3,2,1:T(8,128)(2,1)S(1)} %get-tuple-element.290), kind=kOutput, calls=%fused_computation.6.clone.1 | convolution fusion | flops 412087296 | bytes 14430208 | tf_op jit(solution)/shard_map/while/body/eval_jaxpr/ihcd,jhcd->ihcj/dot_general | solution.py:44
  207.0 6.8 %fusion.88 = f32[384,4,2]{0,2,1:T(2,128)S(1)} fusion(f32[4,2,1024,384]{3,2,1,0:T(8,128)} %get-tuple-element.257, f32[384,4,2]{0,2,1:T(2,128)S(1)} %fusion.87, pred[384,1024]{0,1:T(8,128)(4,1)S(1)} %broadcast_compare_fusion.2), kind=kLoop, calls=%fused_computation.8.clone.1 | loop fusion | flops 15725568 | bytes 13000704 | tf_op jit(solution)/shard_map/while/body/eval_jaxpr/reduce_sum | solution.py:55
  213.9 1.4 copy-done
  215.3 3.6 %bitcast_add_fusion.2 = f32[384,4,2,128]{0,3,2,1:T(8,128)S(1)} fusion(f32[384,4,2,128]{0,3,2,1:T(8,128)S(1)} %get-tuple-element.276, bf16[1024,4,128,1]{0,2,3,1:T(8,128)(2,1)S(1)} %bitcast.149, f32[4,2,1024,384]{3,2,1,0:T(8,128)S(1)} %copy-done, f32[384,4,2]{0,2,1:T(2,128)S(1)} %fusion.87, pred[384,1024]{0,1:T(8,128)(4,1)S(1)} %broadcast_compare_fusion.2, ...), kind=kOutput, calls=%fused_computation.11.clone.1 | convolution fusion | flops 822214656 | bytes 17195008 | tf_op jit(solution)/shard_map/while/body/eval_jaxpr/ihcj,jhe->ihce/dot_general | solution.py:56
  218.9 0.3 broadcast_compare_fusion.2
  219.2 1.7 constant_dynamic-slice_fusion.3
  220.9 6.7 %fusion.86 = (f32[384,4,2]{0,2,1:T(2,128)S(1)}, f32[4,2,1024,384]{3,2,1,0:T(8,128)}) fusion(pred[384,1024]{0,1:T(8,128)(4,1)S(1)} %broadcast_compare_fusion.2, bf16[1024,4,2,64]{0,3,2,1:T(8,128)(2,1)S(1)} %bitcast.148, bf16[384,4,2,64]{0,3,2,1:T(8,128)(2,1)S(1)} %get-tuple-element.290), kind=kOutput, calls=%fused_computation.6.clone.1 | convolution fusion | flops 412087296 | bytes 14430208 | tf_op jit(solution)/shard_map/while/body/eval_jaxpr/ihcd,jhcd->ihcj/dot_general | solution.py:44
  227.6 6.8 %fusion.88 = f32[384,4,2]{0,2,1:T(2,128)S(1)} fusion(f32[4,2,1024,384]{3,2,1,0:T(8,128)} %get-tuple-element.257, f32[384,4,2]{0,2,1:T(2,128)S(1)} %fusion.87, pred[384,1024]{0,1:T(8,128)(4,1)S(1)} %broadcast_compare_fusion.2), kind=kLoop, calls=%fused_computation.8.clone.1 | loop fusion | flops 15725568 | bytes 13000704 | tf_op jit(solution)/shard_map/while/body/eval_jaxpr/reduce_sum | solution.py:55
  234.4 1.4 copy-done
  235.9 3.6 %bitcast_add_fusion.2 = f32[384,4,2,128]{0,3,2,1:T(8,128)S(1)} fusion(f32[384,4,2,128]{0,3,2,1:T(8,128)S(1)} %get-tuple-element.276, bf16[1024,4,128,1]{0,2,3,1:T(8,128)(2,1)S(1)} %bitcast.149, f32[4,2,1024,384]{3,2,1,0:T(8,128)S(1)} %copy-done, f32[384,4,2]{0,2,1:T(2,128)S(1)} %fusion.87, pred[384,1024]{0,1:T(8,128)(4,1)S(1)} %broadcast_compare_fusion.2, ...), kind=kOutput, calls=%fused_computation.11.clone.1 | convolution fusion | flops 822214656 | bytes 17195008 | tf_op jit(solution)/shard_map/while/body/eval_jaxpr/ihcj,jhe->ihce/dot_general | solution.py:56
  239.5 0.1 broadcast_divide_fusion
  239.6 0.2 fusion.64
  239.8 0.1 fusion.69
  239.9 0.1 mul.183
  240.0 1.0 multiply_convert_fusion
  241.0 0.0 all-gather.14.cloned.1.call-done
  241.0 6.1 %fusion.38 = bf16[8,1,64,1024]{3,2,1,0:T(8,128)(2,1)} fusion(bf16[1,2048,1024]{2,1,0:T(8,128)(2,1)} %param.27, bf16[8,1,64,2048]{3,2,0,1:T(8,128)(2,1)} %all-gather.14.cloned.1.call-done), kind=kOutput, calls=%fused_computation.43 | convolution fusion | flops 2148007936 | bytes 7340032 | tf_op jit(solution)/shard_map/sxcf,xfd->sxcd/dot_general | solution.py:124
  247.2 3.6 %all-to-all-start.1 = ((bf16[8,1,64,1024]{3,2,1,0:T(8,128)(2,1)}), bf16[8,1,64,1024]{3,2,1,0:T(8,128)(2,1)S(1)}, u32[]{:S(2)}, u32[]{:S(2)}) async-start(bf16[8,1,64,1024]{3,2,1,0:T(8,128)(2,1)} %fusion.38), calls=%async_computation.1 | async-start | bytes 2097152 | tf_op jit(solution)/shard_map/all_to_all | solution.py:131
  250.7 0.1 copy.40
  250.9 20.8 %all-gather.10.cloned.1.call-done = bf16[1,1,384,2048]{2,3,1,0:T(8,128)(2,1)} async-done(((bf16[1,1,384,512]{2,3,1,0:T(8,128)(2,1)}), bf16[1,1,384,2048]{2,3,1,0:T(8,128)(2,1)}) %all-gather.10.cloned.1.call-update) | async-done | bytes 1572880 | tf_op jit(solution)/shard_map/all_gather | solution.py:117
  271.6 5.4 %fusion.35 = bf16[384,1024]{1,0:T(8,128)(2,1)} fusion(bf16[2048,1024]{1,0:T(8,128)(2,1)} %param.20, bf16[1,1,384,2048]{2,3,1,0:T(8,128)(2,1)} %all-gather.10.cloned.1.call-done), kind=kOutput, calls=%fused_computation.42 | convolution fusion | flops 1611005952 | bytes 6553600 | tf_op jit(solution)/shard_map/dot_general | solution.py:116
  277.0 0.2 all-to-all-done.1
  277.2 1.2 gather_fusion.1
  278.4 0.7 reshape.247
  279.0 2.1 multiply_reduce_fusion
  (50 shorter events, 0.4 us)
Async XLA Ops:
  7.2 92.2 %all-gather.12.cloned.1.call-start = ((), (), s32[]{:S(2)}) async-start(), calls=%async_computation.5 | async-start | bytes 5242880 | tf_op jit(solution)/shard_map/all_gather | solution.py:109
  12.6 35.1 %copy-start.2 = (bf16[384,512]{1,0:T(8,128)(2,1)S(1)}, bf16[384,512]{1,0:T(8,128)(2,1)}, u32[]{:S(2)}) copy-start(bf16[384,512]{1,0:T(8,128)(2,1)} %param.16) | copy-start | bytes 1179652
  14.7 34.1 %copy-start.3 = (bf16[384,512]{1,0:T(8,128)(2,1)S(1)}, bf16[384,512]{1,0:T(8,128)(2,1)}, u32[]{:S(2)}) copy-start(bf16[384,512]{1,0:T(8,128)(2,1)} %param.17) | copy-start | bytes 1179652
  14.7 36.3 %copy-start.4 = (f32[4]{0:T(128)S(1)}, f32[4]{0:T(128)}, u32[]{:S(2)}) copy-start(f32[4]{0:T(128)} %param.18) | copy-start | bytes 52
  14.7 36.3 %copy-start.6 = (f32[128]{0:T(128)S(1)}, f32[128]{0:T(128)}, u32[]{:S(2)}) copy-start(f32[128]{0:T(128)} %param.19) | copy-start | bytes 1540
  47.7 54.9 %copy-start.8 = (f32[4096]{0:T(1024)S(1)}, f32[4096]{0:T(1024)}, u32[]{:S(2)}) copy-start(f32[4096]{0:T(1024)} %param.22) | copy-start | bytes 49156
  47.7 91.1 %all-gather.6.cloned.1.call-start = ((), (), s32[]{:S(2)}) async-start(), calls=%async_computation.2 | async-start | bytes 3538944 | tf_op jit(solution)/shard_map/all_gather | solution.py:69
  48.7 128.8 %all-gather.8.cloned.1.call-start = ((), (), s32[]{:S(2)}) async-start(), calls=%async_computation.3 | async-start | bytes 3538944 | tf_op jit(solution)/shard_map/all_gather | solution.py:70
  49.7 191.3 %all-gather.14.cloned.1.call-start = ((), (), s32[]{:S(2)}) async-start(), calls=%async_computation.6 | async-start | bytes 2621440 | tf_op jit(solution)/shard_map/all_gather | solution.py:126
  99.3 3.4 %copy-start.1 = (bf16[8,1,64,4096]{3,2,1,0:T(8,128)(2,1)S(1)}, bf16[8,1,64,4096]{3,2,1,0:T(8,128)(2,1)}, u32[]{:S(2)}) copy-start(bf16[8,1,64,4096]{3,2,1,0:T(8,128)(2,1)} %all-gather.12.cloned.1.call-done) | copy-start | bytes 12582916
  102.8 4.7 %copy-start.7 = (bf16[1,4096,512]{2,1,0:T(8,128)(2,1)S(1)}, bf16[1,4096,512]{2,1,0:T(8,128)(2,1)}, u32[]{:S(2)}) copy-start(bf16[1,4096,512]{2,1,0:T(8,128)(2,1)} %param.26) | copy-start | bytes 12582916
  110.8 160.8 %all-gather.10.cloned.1.call-start = ((), (), s32[]{:S(2)}) async-start(), calls=%async_computation.4 | async-start | bytes 1966080 | tf_op jit(solution)/shard_map/all_gather | solution.py:117
  186.2 8.5 %copy-start = (f32[4,2,1024,384]{3,2,1,0:T(8,128)S(1)}, f32[4,2,1024,384]{3,2,1,0:T(8,128)}, u32[]{:S(2)}) copy-start(f32[4,2,1024,384]{3,2,1,0:T(8,128)} %get-tuple-element.257) | copy-start | bytes 37748740 | tf_op jit(solution)/shard_map/while
  207.0 8.3 %copy-start = (f32[4,2,1024,384]{3,2,1,0:T(8,128)S(1)}, f32[4,2,1024,384]{3,2,1,0:T(8,128)}, u32[]{:S(2)}) copy-start(f32[4,2,1024,384]{3,2,1,0:T(8,128)} %get-tuple-element.257) | copy-start | bytes 37748740 | tf_op jit(solution)/shard_map/while
  227.6 8.3 %copy-start = (f32[4,2,1024,384]{3,2,1,0:T(8,128)S(1)}, f32[4,2,1024,384]{3,2,1,0:T(8,128)}, u32[]{:S(2)}) copy-start(f32[4,2,1024,384]{3,2,1,0:T(8,128)} %get-tuple-element.257) | copy-start | bytes 37748740 | tf_op jit(solution)/shard_map/while
  241.0 9.7 %copy-start.5 = (f32[128,2]{0,1:T(2,128)S(1)}, f32[128,2]{0,1:T(2,128)}, u32[]{:S(2)}) copy-start(f32[128,2]{0,1:T(2,128)} %param.24) | copy-start | bytes 3076
  247.2 30.1 %all-to-all-start.1 = ((bf16[8,1,64,1024]{3,2,1,0:T(8,128)(2,1)}), bf16[8,1,64,1024]{3,2,1,0:T(8,128)(2,1)S(1)}, u32[]{:S(2)}, u32[]{:S(2)}) async-start(bf16[8,1,64,1024]{3,2,1,0:T(8,128)(2,1)} %fusion.38), calls=%async_computation.1 | async-start | bytes 2097152 | tf_op jit(solution)/shard_map/all_to_all | solution.py:131
Sparse Core Ops, SparseCore 0:
  47.8 51.4 all-gather.11
  101.0 37.7 all-gather.5
  140.4 37.0 all-gather.7
  179.8 34.3 all-gather.13
  241.1 30.4 all-gather.9
where the time goes:
time: 288 us
  waiting for transfers between devices  136 us (47%)
  matrix products  50.1 us (17%)
  blocking collectives  33 us (11%)
  other arithmetic  29.5 us (10%)
  local copies, waits for them, and re-layouts  21 us (7%)
  between operations  14 us (5%)
  starting transfers between devices  3.94 us (1%)
    all_gather x1, waiting for transfers between devices, per_device(): lax.all_gather(column_parts, 'tp', axis=3, tiled=True)  48.2 us
    all_gather x1, waiting for transfers between devices, per_device(): value_part = lax.all_gather(value_rows, 'ep', axis=0, tiled=True)  38.8 us
    all_to_all x1, blocking collectives, per_device(): lax.all_to_all(outgoing, 'ep', split_axis=0, concat_axis=0, tiled=True)  33 us
    all_gather x1, waiting for transfers between devices, per_device(): key_part = lax.all_gather(key_rows, 'ep', axis=0, tiled=True)  27.7 us
    all_gather x1, waiting for transfers between devices, per_device(): lax.all_gather(head_out.reshape(1, 1, count_a, head_out.shape[1]), 'tp',...  20.8 us
    reduce_sum x3, other arithmetic, key_block(): new_sum = old_sum * shrink + jnp.sum(weights, axis=-1)  20.5 us
    dot_general x3, matrix products, key_block(): jnp.einsum('ihcd,jhcd->ihcj', query_four, key_four, preferred_element_typ...  20 us
    dot_general x3, matrix products, key_block(): jnp.einsum('ihcj,jhe->ihce', weights.astype(jnp.bfloat16), value_three, p...  10.7 us
  transfers between devices with their start and end apart: 6, of which 5 were waited for; matrix products, arithmetic and copies ran while one was open for 29% of the time, Pallas kernels for 0%

commit v1 on v0

--- a/solution.py
+++ b/solution.py
@@ -66,8 +66,10 @@
         jnp.zeros((count_a, per_head, 2), jnp.float32),
         jnp.zeros((count_a, per_head, 2, value_dim), jnp.float32),
     )
-    key_part = lax.all_gather(key_rows, "ep", axis=0, tiled=True)
-    value_part = lax.all_gather(value_rows, "ep", axis=0, tiled=True)
+    current_block = jnp.concatenate([key_rows, value_rows], axis=1)
+    key_part, value_part = jnp.split(
+        lax.all_gather(current_block, "ep", axis=0, tiled=True), [key_rows.shape[1]], axis=1
+    )
     key_count = key_part.shape[0]
 
     def step_block(block_num, inner_state):

time: 288 us -> 288 us (level)
  waiting for transfers between devices: 136 us -> 130 us
  local copies, waits for them, and re-layouts: 21 us -> 25.7 us
    all_to_all x1, waiting for transfers between devices: 0.23 us -> 26.4 us  [per_device(): lax.all_to_all(moe_total.astype(jnp.bfloat16), 'ep', split_axis=0, concat...]
    all_gather x1, waiting for transfers between devices: 20.8 us -> 0.01 us  [per_device(): lax.all_gather(head_out.reshape(1, 1, count_a, head_out.shape[1]), 'tp',...]
    all_gather x2 -> x1, waiting for transfers between devices: 66.5 us -> 55 us  [per_device(): lax.all_gather(current_block, 'ep', axis=0, tiled=True)]
    split x0 -> x1, local copies, waits for them, and re-layouts: none -> 5.88 us  [per_device(): jnp.split(lax.all_gather(current_block, 'ep', axis=0, tiled=True), [key_r...]
  transfers between devices with their start and end apart: 6 -> 5, of which waited for: 5 -> 3; matrix products, arithmetic and copies ran while one was open for 29% -> 31% of each run, Pallas kernels for 0% -> 0%
where the time goes in v1:
time: 288 us
  waiting for transfers between devices  130 us (45%)
  matrix products  50.4 us (18%)
  blocking collectives  33 us (11%)
  other arithmetic  30.3 us (11%)
  local copies, waits for them, and re-layouts  25.7 us (9%)
  between operations  14 us (5%)
  starting transfers between devices  3.9 us (1%)
    all_gather x1, waiting for transfers between devices, per_device(): lax.all_gather(current_block, 'ep', axis=0, tiled=True)  55 us
    all_gather x1, waiting for transfers between devices, per_device(): lax.all_gather(column_parts, 'tp', axis=3, tiled=True)  48.8 us
    all_to_all x1, blocking collectives, per_device(): lax.all_to_all(outgoing, 'ep', split_axis=0, concat_axis=0, tiled=True)  33 us
    all_to_all x1, waiting for transfers between devices, per_device(): lax.all_to_all(moe_total.astype(jnp.bfloat16), 'ep', split_axis=0, concat...  26.4 us
    reduce_sum x3, other arithmetic, key_block(): new_sum = old_sum * shrink + jnp.sum(weights, axis=-1)  20.3 us
    dot_general x3, matrix products, key_block(): jnp.einsum('ihcd,jhcd->ihcj', query_four, key_four, preferred_element_typ...  20 us
    dot_general x3, matrix products, key_block(): jnp.einsum('ihcj,jhe->ihce', weights.astype(jnp.bfloat16), value_three, p...  10.9 us
    dot_general x1, matrix products, per_device(): jnp.einsum('sxcf,xfd->sxcd', lax.all_gather(hidden, 'tp', axis=3, tiled=T...  6.13 us
  transfers between devices with their start and end apart: 5, of which 3 were waited for; matrix products, arithmetic and copies ran while one was open for 31% of the time, Pallas kernels for 0%

profile of v1, /device:TPU:0, one launch (start us, length us, event | category | flops | bytes accessed | tf_op | source)
XLA Modules:
  0.0 287.6 jit_solution(18112408570983247478)
XLA Ops:
  7.2 0.0 all-gather.9.cloned.1.call-start
  7.2 0.7 broadcast_multiply_fusion
  7.9 0.8 copy.36
  8.7 0.1 eq.29
  8.8 0.1 eq.25
  9.0 0.1 copy.35
  9.1 0.1 mul.194
  9.2 0.6 reduce-window.6
  9.8 0.2 slice_reduce_fusion
  10.1 0.1 fusion.65
  10.2 1.4 scatter_custom_fusion
  11.6 1.0 concatenate.7
  12.6 2.1 gather_fusion
  14.7 33.0 %all_to_all.10 = bf16[8,1,64,1024]{3,2,1,0:T(8,128)(2,1)} all-to-all(bf16[8,1,64,1024]{3,2,1,0:T(8,128)(2,1)S(1)} %bitcast.152), channel_id=1, replica_groups=mesh['ep'=8,'tp'=4] {'ep'}, dimensions={0} | all-to-all | bytes 2097152 | tf_op jit(solution)/shard_map/all_to_all | solution.py:110
  47.7 0.0 all-gather.9.cloned.1.call-update
  47.7 0.0 all-gather.5.cloned.1.call-start
  47.7 0.2 copy.32
  48.0 0.2 copy.31
  48.2 1.0 pad_maximum_fusion
  49.2 0.0 all-gather.5.cloned.1.call-update
  49.2 0.0 all-gather.11.cloned.1.call-start
  49.3 1.2 copy.33
  50.5 0.1 broadcast_bitcast_fusion
  50.6 48.8 %all-gather.9.cloned.1.call-done = bf16[8,1,64,4096]{3,2,1,0:T(8,128)(2,1)} async-done(((bf16[8,1,64,1024]{3,2,1,0:T(8,128)(2,1)}), bf16[8,1,64,4096]{3,2,1,0:T(8,128)(2,1)}) %all-gather.9.cloned.1.call-update) | async-done | bytes 4194320 | tf_op jit(solution)/shard_map/all_gather | solution.py:111
  99.3 3.2 %fusion.15 = f32[8,64]{1,0:T(8,128)S(1)} fusion(bf16[8,1,64,4096]{3,2,1,0:T(8,128)(2,1)} %all-gather.9.cloned.1.call-done), kind=kLoop, calls=%fused_computation.28 | loop fusion | flops 6290944 | bytes 4196352 | tf_op jit(solution)/shard_map/reduce_sum | solution.py:14
  102.6 0.2 copy-done.1
  102.8 4.7 %fusion.43 = f32[8,1,64,512]{3,2,0,1:T(8,128)S(1)} fusion(bf16[1,4096,512]{2,1,0:T(8,128)(2,1)} %param.25, bf16[8,1,64,4096]{3,2,1,0:T(8,128)(2,1)S(1)} %copy-done.1, f32[4096]{0:T(1024)S(1)} %copy-done.8, f32[8,64]{1,0:T(8,128)S(1)} %add_rsqrt_fusion.1), kind=kOutput, calls=%fused_computation.44 | convolution fusion | flops 2155872256 | bytes 9455616 | tf_op jit(solution)/shard_map/sxcd,xdf->sxcf/dot_general | solution.py:112
  107.5 3.3 %fusion.58 = bf16[8,1,64,512]{3,2,0,1:T(8,128)(2,1)} fusion(bf16[1,4096,512]{2,1,0:T(8,128)(2,1)S(1)} %copy-done.7, bf16[8,1,64,4096]{3,2,1,0:T(8,128)(2,1)S(1)} %copy-done.1, f32[4096]{0:T(1024)S(1)} %copy-done.8, f32[8,64]{1,0:T(8,128)S(1)} %add_rsqrt_fusion.1, f32[8,1,64,512]{3,2,0,1:T(8,128)S(1)} %fusion.43), kind=kOutput, calls=%fused_computation.47 | convolution fusion | flops 2157445120 | bytes 9979904 | tf_op jit(solution)/shard_map/sxcd,xdf->sxcf/dot_general | solution.py:115
  110.8 0.2 all-gather.7.cloned.1.call-start
  111.0 55.0 %all-gather.5.cloned.1.call-done = bf16[3072,1024]{0,1:T(8,128)(2,1)} async-done(((bf16[384,1024]{0,1:T(8,128)(2,1)}), bf16[3072,1024]{0,1:T(8,128)(2,1)}) %all-gather.5.cloned.1.call-update) | async-done | bytes 6291472 | tf_op jit(solution)/shard_map/all_gather | solution.py:71
  166.0 5.9 %fusion.69 = (bf16[3072,512]{0,1:T(8,128)(2,1)}, bf16[3072,512]{0,1:T(8,128)(2,1)}) fusion(bf16[3072,1024]{0,1:T(8,128)(2,1)} %all-gather.5.cloned.1.call-done), kind=kLoop, calls=%fused_computation.77 | loop fusion | bytes 12582912 | tf_op jit(solution)/shard_map/split | solution.py:70
  171.9 62.2 %while.18 = (s32[]{:T(128)}, f32[384,4,2]{0,2,1:T(2,128)S(1)}, f32[384,4,2]{0,2,1:T(2,128)S(1)}, f32[384,4,2,128]{0,3,2,1:T(8,128)S(1)}, bf16[3072,512]{0,1:T(8,...) while((s32[]{:T(128)}, f32[384,4,2]{0,2,1:T(2,128)S(1)}, ...), condition=%wide.region_3.4_spmd.clone, body=%wide.region_0.3_spmd.clone.sunk | while | flops 1250443648 | bytes 99691744 | solution.py:81
  171.9 0.3 broadcast_compare_fusion.2
  172.2 1.9 constant_dynamic-slice_fusion.3
  174.0 6.7 %fusion.87 = (f32[384,4,2]{0,2,1:T(2,128)S(1)}, f32[4,2,1024,384]{3,2,1,0:T(8,128)}) fusion(pred[384,1024]{0,1:T(8,128)(4,1)S(1)} %broadcast_compare_fusion.2, bf16[1024,4,2,64]{0,3,2,1:T(8,128)(2,1)S(1)} %bitcast.148, bf16[384,4,2,64]{0,3,2,1:T(8,128)(2,1)S(1)} %get-tuple-element.292), kind=kOutput, calls=%fused_computation.6.clone.1 | convolution fusion | flops 412087296 | bytes 14430208 | tf_op jit(solution)/shard_map/while/body/eval_jaxpr/ihcd,jhcd->ihcj/dot_general | solution.py:44
  180.7 6.8 %fusion.89 = f32[384,4,2]{0,2,1:T(2,128)S(1)} fusion(f32[4,2,1024,384]{3,2,1,0:T(8,128)} %get-tuple-element.259, f32[384,4,2]{0,2,1:T(2,128)S(1)} %fusion.88, pred[384,1024]{0,1:T(8,128)(4,1)S(1)} %broadcast_compare_fusion.2), kind=kLoop, calls=%fused_computation.8.clone.1 | loop fusion | flops 15725568 | bytes 13000704 | tf_op jit(solution)/shard_map/while/body/eval_jaxpr/reduce_sum | solution.py:55
  187.6 1.6 copy-done
  189.1 3.6 %bitcast_add_fusion.2 = f32[384,4,2,128]{0,3,2,1:T(8,128)S(1)} fusion(f32[384,4,2,128]{0,3,2,1:T(8,128)S(1)} %get-tuple-element.278, bf16[1024,4,128,1]{0,2,3,1:T(8,128)(2,1)S(1)} %bitcast.149, f32[4,2,1024,384]{3,2,1,0:T(8,128)S(1)} %copy-done, f32[384,4,2]{0,2,1:T(2,128)S(1)} %fusion.88, pred[384,1024]{0,1:T(8,128)(4,1)S(1)} %broadcast_compare_fusion.2, ...), kind=kOutput, calls=%fused_computation.11.clone.1 | convolution fusion | flops 822214656 | bytes 17195008 | tf_op jit(solution)/shard_map/while/body/eval_jaxpr/ihcj,jhe->ihce/dot_general | solution.py:56
  192.8 0.3 broadcast_compare_fusion.2
  193.1 1.7 constant_dynamic-slice_fusion.3
  194.8 6.7 %fusion.87 = (f32[384,4,2]{0,2,1:T(2,128)S(1)}, f32[4,2,1024,384]{3,2,1,0:T(8,128)}) fusion(pred[384,1024]{0,1:T(8,128)(4,1)S(1)} %broadcast_compare_fusion.2, bf16[1024,4,2,64]{0,3,2,1:T(8,128)(2,1)S(1)} %bitcast.148, bf16[384,4,2,64]{0,3,2,1:T(8,128)(2,1)S(1)} %get-tuple-element.292), kind=kOutput, calls=%fused_computation.6.clone.1 | convolution fusion | flops 412087296 | bytes 14430208 | tf_op jit(solution)/shard_map/while/body/eval_jaxpr/ihcd,jhcd->ihcj/dot_general | solution.py:44
  201.5 6.8 %fusion.89 = f32[384,4,2]{0,2,1:T(2,128)S(1)} fusion(f32[4,2,1024,384]{3,2,1,0:T(8,128)} %get-tuple-element.259, f32[384,4,2]{0,2,1:T(2,128)S(1)} %fusion.88, pred[384,1024]{0,1:T(8,128)(4,1)S(1)} %broadcast_compare_fusion.2), kind=kLoop, calls=%fused_computation.8.clone.1 | loop fusion | flops 15725568 | bytes 13000704 | tf_op jit(solution)/shard_map/while/body/eval_jaxpr/reduce_sum | solution.py:55
  208.3 1.4 copy-done
  209.8 3.6 %bitcast_add_fusion.2 = f32[384,4,2,128]{0,3,2,1:T(8,128)S(1)} fusion(f32[384,4,2,128]{0,3,2,1:T(8,128)S(1)} %get-tuple-element.278, bf16[1024,4,128,1]{0,2,3,1:T(8,128)(2,1)S(1)} %bitcast.149, f32[4,2,1024,384]{3,2,1,0:T(8,128)S(1)} %copy-done, f32[384,4,2]{0,2,1:T(2,128)S(1)} %fusion.88, pred[384,1024]{0,1:T(8,128)(4,1)S(1)} %broadcast_compare_fusion.2, ...), kind=kOutput, calls=%fused_computation.11.clone.1 | convolution fusion | flops 822214656 | bytes 17195008 | tf_op jit(solution)/shard_map/while/body/eval_jaxpr/ihcj,jhe->ihce/dot_general | solution.py:56
  213.5 0.3 broadcast_compare_fusion.2
  213.8 1.7 constant_dynamic-slice_fusion.3
  215.5 6.7 %fusion.87 = (f32[384,4,2]{0,2,1:T(2,128)S(1)}, f32[4,2,1024,384]{3,2,1,0:T(8,128)}) fusion(pred[384,1024]{0,1:T(8,128)(4,1)S(1)} %broadcast_compare_fusion.2, bf16[1024,4,2,64]{0,3,2,1:T(8,128)(2,1)S(1)} %bitcast.148, bf16[384,4,2,64]{0,3,2,1:T(8,128)(2,1)S(1)} %get-tuple-element.292), kind=kOutput, calls=%fused_computation.6.clone.1 | convolution fusion | flops 412087296 | bytes 14430208 | tf_op jit(solution)/shard_map/while/body/eval_jaxpr/ihcd,jhcd->ihcj/dot_general | solution.py:44
  222.2 6.8 %fusion.89 = f32[384,4,2]{0,2,1:T(2,128)S(1)} fusion(f32[4,2,1024,384]{3,2,1,0:T(8,128)} %get-tuple-element.259, f32[384,4,2]{0,2,1:T(2,128)S(1)} %fusion.88, pred[384,1024]{0,1:T(8,128)(4,1)S(1)} %broadcast_compare_fusion.2), kind=kLoop, calls=%fused_computation.8.clone.1 | loop fusion | flops 15725568 | bytes 13000704 | tf_op jit(solution)/shard_map/while/body/eval_jaxpr/reduce_sum | solution.py:55
  229.0 1.4 copy-done
  230.5 3.6 %bitcast_add_fusion.2 = f32[384,4,2,128]{0,3,2,1:T(8,128)S(1)} fusion(f32[384,4,2,128]{0,3,2,1:T(8,128)S(1)} %get-tuple-element.278, bf16[1024,4,128,1]{0,2,3,1:T(8,128)(2,1)S(1)} %bitcast.149, f32[4,2,1024,384]{3,2,1,0:T(8,128)S(1)} %copy-done, f32[384,4,2]{0,2,1:T(2,128)S(1)} %fusion.88, pred[384,1024]{0,1:T(8,128)(4,1)S(1)} %broadcast_compare_fusion.2, ...), kind=kOutput, calls=%fused_computation.11.clone.1 | convolution fusion | flops 822214656 | bytes 17195008 | tf_op jit(solution)/shard_map/while/body/eval_jaxpr/ihcj,jhe->ihce/dot_general | solution.py:56
  234.1 0.1 broadcast_divide_fusion
  234.2 0.2 fusion.64
  234.4 0.1 fusion.70
  234.5 0.1 mul.183
  234.6 1.0 multiply_convert_fusion
  235.6 0.0 all-gather.11.cloned.1.call-done
  235.7 6.1 %fusion.38 = bf16[8,1,64,1024]{3,2,1,0:T(8,128)(2,1)} fusion(bf16[1,2048,1024]{2,1,0:T(8,128)(2,1)} %param.27, bf16[8,1,64,2048]{3,2,0,1:T(8,128)(2,1)} %all-gather.11.cloned.1.call-done), kind=kOutput, calls=%fused_computation.43 | convolution fusion | flops 2148007936 | bytes 7340032 | tf_op jit(solution)/shard_map/sxcf,xfd->sxcd/dot_general | solution.py:126
  241.8 3.6 %all-to-all-start.1 = ((bf16[8,1,64,1024]{3,2,1,0:T(8,128)(2,1)}), bf16[8,1,64,1024]{3,2,1,0:T(8,128)(2,1)S(1)}, u32[]{:S(2)}, u32[]{:S(2)}) async-start(bf16[8,1,64,1024]{3,2,1,0:T(8,128)(2,1)} %fusion.38), calls=%async_computation.1 | async-start | bytes 2097152 | tf_op jit(solution)/shard_map/all_to_all | solution.py:133
  245.4 0.1 copy.40
  245.5 26.4 %all-to-all-done.1 = bf16[8,1,64,1024]{3,2,1,0:T(8,128)(2,1)S(1)} async-done(((bf16[8,1,64,1024]{3,2,1,0:T(8,128)(2,1)}), bf16[8,1,64,1024]{3,2,1,0:T(8,128)(2,1)S(1)}, u32[]{:S(2)}, u32[]{:S(2)}) %all-to-all-start.1) | async-done | bytes 1048608 | tf_op jit(solution)/shard_map/all_to_all | solution.py:133
  271.8 1.2 gather_fusion.1
  273.0 0.7 reshape.247
  273.7 2.1 multiply_reduce_fusion
  275.7 5.4 %fusion.35 = bf16[384,1024]{1,0:T(8,128)(2,1)} fusion(bf16[2048,1024]{1,0:T(8,128)(2,1)} %param.20, bf16[1,1,384,2048]{2,3,1,0:T(8,128)(2,1)} %all-gather.7.cloned.1.call-done), kind=kOutput, calls=%fused_computation.42 | convolution fusion | flops 1611005952 | bytes 6553600 | tf_op jit(solution)/shard_map/dot_general | solution.py:118
  (49 shorter events, 0.4 us)
Async XLA Ops:
  7.2 92.2 %all-gather.9.cloned.1.call-start = ((), (), s32[]{:S(2)}) async-start(), calls=%async_computation.4 | async-start | bytes 5242880 | tf_op jit(solution)/shard_map/all_gather | solution.py:111
  12.6 35.1 %copy-start.2 = (bf16[384,512]{1,0:T(8,128)(2,1)S(1)}, bf16[384,512]{1,0:T(8,128)(2,1)}, u32[]{:S(2)}) copy-start(bf16[384,512]{1,0:T(8,128)(2,1)} %param.17) | copy-start | bytes 1179652
  14.7 33.3 %copy-start.3 = (bf16[384,512]{1,0:T(8,128)(2,1)S(1)}, bf16[384,512]{1,0:T(8,128)(2,1)}, u32[]{:S(2)}) copy-start(bf16[384,512]{1,0:T(8,128)(2,1)} %param.16) | copy-start | bytes 1179652
  14.7 35.8 %copy-start.4 = (f32[4]{0:T(128)S(1)}, f32[4]{0:T(128)}, u32[]{:S(2)}) copy-start(f32[4]{0:T(128)} %param.18) | copy-start | bytes 52
  14.7 35.8 %copy-start.6 = (f32[128]{0:T(128)S(1)}, f32[128]{0:T(128)}, u32[]{:S(2)}) copy-start(f32[128]{0:T(128)} %param.19) | copy-start | bytes 1540
  47.7 118.3 %all-gather.5.cloned.1.call-start = ((), (), s32[]{:S(2)}) async-start(), calls=%async_computation.2 | async-start | bytes 7077888 | tf_op jit(solution)/shard_map/all_gather | solution.py:71
  48.0 54.6 %copy-start.8 = (f32[4096]{0:T(1024)S(1)}, f32[4096]{0:T(1024)}, u32[]{:S(2)}) copy-start(f32[4096]{0:T(1024)} %param.22) | copy-start | bytes 49156
  49.2 186.5 %all-gather.11.cloned.1.call-start = ((), (), s32[]{:S(2)}) async-start(), calls=%async_computation.5 | async-start | bytes 2621440 | tf_op jit(solution)/shard_map/all_gather | solution.py:128
  99.3 3.4 %copy-start.1 = (bf16[8,1,64,4096]{3,2,1,0:T(8,128)(2,1)S(1)}, bf16[8,1,64,4096]{3,2,1,0:T(8,128)(2,1)}, u32[]{:S(2)}) copy-start(bf16[8,1,64,4096]{3,2,1,0:T(8,128)(2,1)} %all-gather.9.cloned.1.call-done) | copy-start | bytes 12582916
  102.8 4.7 %copy-start.7 = (bf16[1,4096,512]{2,1,0:T(8,128)(2,1)S(1)}, bf16[1,4096,512]{2,1,0:T(8,128)(2,1)}, u32[]{:S(2)}) copy-start(bf16[1,4096,512]{2,1,0:T(8,128)(2,1)} %param.26) | copy-start | bytes 12582916
  110.8 164.9 %all-gather.7.cloned.1.call-start = ((), (), s32[]{:S(2)}) async-start(), calls=%async_computation.3 | async-start | bytes 1966080 | tf_op jit(solution)/shard_map/all_gather | solution.py:119
  180.7 8.4 %copy-start = (f32[4,2,1024,384]{3,2,1,0:T(8,128)S(1)}, f32[4,2,1024,384]{3,2,1,0:T(8,128)}, u32[]{:S(2)}) copy-start(f32[4,2,1024,384]{3,2,1,0:T(8,128)} %get-tuple-element.259) | copy-start | bytes 37748740 | tf_op jit(solution)/shard_map/while
  201.5 8.3 %copy-start = (f32[4,2,1024,384]{3,2,1,0:T(8,128)S(1)}, f32[4,2,1024,384]{3,2,1,0:T(8,128)}, u32[]{:S(2)}) copy-start(f32[4,2,1024,384]{3,2,1,0:T(8,128)} %get-tuple-element.259) | copy-start | bytes 37748740 | tf_op jit(solution)/shard_map/while
  222.2 8.3 %copy-start = (f32[4,2,1024,384]{3,2,1,0:T(8,128)S(1)}, f32[4,2,1024,384]{3,2,1,0:T(8,128)}, u32[]{:S(2)}) copy-start(f32[4,2,1024,384]{3,2,1,0:T(8,128)} %get-tuple-element.259) | copy-start | bytes 37748740 | tf_op jit(solution)/shard_map/while
  235.6 9.7 %copy-start.5 = (f32[128,2]{0,1:T(2,128)S(1)}, f32[128,2]{0,1:T(2,128)}, u32[]{:S(2)}) copy-start(f32[128,2]{0,1:T(2,128)} %param.24) | copy-start | bytes 3076
  241.8 30.1 %all-to-all-start.1 = ((bf16[8,1,64,1024]{3,2,1,0:T(8,128)(2,1)}), bf16[8,1,64,1024]{3,2,1,0:T(8,128)(2,1)S(1)}, u32[]{:S(2)}, u32[]{:S(2)}) async-start(bf16[8,1,64,1024]{3,2,1,0:T(8,128)(2,1)} %fusion.38), calls=%async_computation.1 | async-start | bytes 2097152 | tf_op jit(solution)/shard_map/all_to_all | solution.py:133
Sparse Core Ops, SparseCore 0:
  47.8 51.4 all-gather.8
  101.5 64.4 all-gather.4
  167.8 33.6 all-gather.10
  235.7 29.1 all-gather.6
